TPU v7x, 32 devices: a whole 2x2x4 slice. The times are simulated.
32 devices in a mesh: ep: 8 (over z, core), tp: 4 (over y, x).
Axes of the slice: x: 2, y: 2, z: 4, core: 2. Of those that a mesh axis runs over, the one named last changes fastest.
Arguments:
- attn_rows: bfloat16 [1024, 2048], P('ep'), may hold values from -6 to 6
- attn_gain: float32 [2048], replicated, may hold values from 0.1 to 1.9
- query_weight: bfloat16 [2048, 1024], P(None, 'tp'), may hold values from -0.125 to 0.125
- key_weight: bfloat16 [2048, 1024], P(None, 'tp'), may hold values from -0.125 to 0.125
- value_weight: bfloat16 [2048, 1024], P(None, 'tp'), may hold values from -0.125 to 0.125
- key_bias: bfloat16 [16, 1024], P('tp', 'ep'), may hold values from -14 to 0
- out_weight: bfloat16 [1024, 2048], P(None, 'tp'), may hold values from -0.75 to 0.75
- expert_rows: bfloat16 [1024, 2048], P('ep'), may hold values from -6 to 6
- expert_gain: float32 [2048], replicated, may hold values from 0.1 to 1.9
- expert_ids: int32 [1024, 2], P('ep'), may hold values from 0 to 31, all different within a row; in each aligned block of 128 rows (0 to 127, 128 to 255, ...) at most 16 rows name the same one
- group_logits: float32 [1024, 4], P('ep'), may hold values from -6 to 6
- pair_logits: float32 [1024, 2], P('ep'), may hold values from -6 to 6
- gate_weight: bfloat16 [32, 2048, 2048], P('ep', None, 'tp'), may hold values from -0.125 to 0.125
- up_weight: bfloat16 [32, 2048, 2048], P('ep', None, 'tp'), may hold values from -0.125 to 0.125
- down_weight: bfloat16 [32, 2048, 2048], P('ep', None, 'tp'), may hold values from -0.125 to 0.125
Outputs:
- mixed: bfloat16 [1024, 2048], P('ep', 'tp')
- expert_out: bfloat16 [1024, 2048], P('ep', 'tp')
Inputs may be any that keep to these rules, and one draw needn't show every extreme that they name: `expert_ids`: each row names two different experts; in every aligned block of 128 rows no expert is named more than 16 times.
All inputs are finite; a program needn't handle non-finite values.
Results may differ from a plain program's by a relative error of at most 0.0083.
Values may be sent and summed in bfloat16 or wider, within the bound.
A program may use at most 64 MiB of HBM per device.

v0:
```python
import jax
import jax.numpy as jnp
from jax import lax
from jax.sharding import PartitionSpec as P

EXPERTS = 32
GROUPS = 4
GROUP_SIZE = 8
CAP = 16
epsilon = 1e-06


def norm_rows(rows, gain):
    values = rows.astype(jnp.float32)
    scaled = values * lax.rsqrt(jnp.mean(values * values, axis=-1, keepdims=True) + epsilon)
    return (scaled * gain).astype(jnp.bfloat16)


def shards(
    attn_rows,
    attn_gain,
    query_weight,
    key_weight,
    value_weight,
    key_bias,
    out_weight,
    expert_rows,
    expert_gain,
    expert_ids,
    group_logits,
    pair_logits,
    gate_weight,
    up_weight,
    down_weight,
):
    rows_dev = attn_rows.shape[0]
    blocks = lax.axis_size("ep")
    own_start = lax.axis_index("ep") * rows_dev
    heads_local = key_bias.shape[0]
    head_size = query_weight.shape[1] // heads_local
    width_local = heads_local * head_size
    scale = head_size ** (-0.5)
    normed = norm_rows(attn_rows, attn_gain)
    query = jnp.dot(normed, query_weight, preferred_element_type=jnp.float32).astype(jnp.bfloat16)
    query = query.reshape(rows_dev, heads_local, head_size)
    keys = jnp.dot(normed, key_weight, preferred_element_type=jnp.float32).astype(jnp.bfloat16)
    values = jnp.dot(normed, value_weight, preferred_element_type=jnp.float32).astype(jnp.bfloat16)
    pairs = jnp.concatenate([keys, values], axis=1)
    bias_rows = key_bias.T
    query_pos = own_start + jnp.arange(rows_dev)
    init = (
        jnp.zeros((blocks, heads_local, rows_dev), jnp.float32),
        jnp.zeros((blocks, heads_local, rows_dev, head_size), jnp.float32),
    )
    piece = (
        lax.all_gather(pairs, "ep", axis=0, tiled=True),
        lax.all_gather(bias_rows, "ep", axis=0, tiled=True),
    )

    def work(state):
        pair_rows, bias_piece = piece
        count = pair_rows.shape[0]
        spans = count // rows_dev
        key_part = pair_rows[:, :width_local].reshape(count, heads_local, head_size)
        value_part = pair_rows[:, width_local:].reshape(spans, rows_dev, heads_local, head_size)
        scores = (
            jnp.einsum("thd,shd->hts", query, key_part, preferred_element_type=jnp.float32) * scale
        )
        scores = scores + bias_piece.T.astype(jnp.float32)[:, None, :]
        scores = scores.reshape(heads_local, rows_dev, spans, rows_dev)
        causal = jnp.arange(count)[None, :] < query_pos[:, None]
        causal = causal.reshape(rows_dev, spans, rows_dev)
        negative_part = jax.nn.log_sigmoid(-scores)
        log_keep = jnp.where(causal, negative_part, 0.0)
        suffix = lax.cumsum(log_keep, axis=3, reverse=True) - log_keep
        weights = jnp.where(causal, jnp.exp(scores + negative_part + suffix), 0.0).astype(
            jnp.bfloat16
        )
        block_out = jnp.einsum(
            "htnr,nrhd->nhtd", weights, value_part, preferred_element_type=jnp.float32
        )
        block_keep = jnp.transpose(jnp.sum(log_keep, axis=3), (2, 0, 1))
        return (block_keep, block_out)

    def untouched(state):
        return state

    totals, outputs = lax.cond(jnp.int32(0) < own_start + rows_dev, work, untouched, init)
    later = lax.cumsum(totals, axis=0, reverse=True) - totals
    merged = jnp.sum(jnp.exp(later)[..., None] * outputs, axis=0)
    attended = jnp.transpose(merged, (1, 0, 2)).reshape(rows_dev, width_local).astype(jnp.bfloat16)
    mixed = jnp.dot(
        lax.all_gather(attended, "tp", axis=1, tiled=True),
        out_weight,
        preferred_element_type=jnp.float32,
    )
    mixed = mixed.astype(jnp.bfloat16)
    normed = norm_rows(expert_rows, expert_gain)
    width = normed.shape[1]
    cols_local = down_weight.shape[2]
    flattened = expert_ids.reshape(-1)
    picks = flattened.shape[0]
    marks = (flattened[:, None] == jnp.arange(EXPERTS)[None, :]).astype(jnp.int32)
    position = jnp.sum((jnp.cumsum(marks, axis=0) - marks) * marks, axis=1)
    source = jnp.arange(picks) // 2
    send = (
        jnp.zeros((EXPERTS, CAP, width), jnp.bfloat16).at[flattened, position].set(normed[source])
    )
    send = send.reshape(blocks, EXPERTS // blocks, CAP, width)
    shares = jnp.exp(group_logits)
    shares = shares / jnp.sum(shares, axis=1, keepdims=True)
    groups = expert_ids // GROUP_SIZE
    group_marks = (groups[:, :, None] == jnp.arange(GROUPS)[None, None, :]).astype(jnp.float32)
    chosen = jnp.sum(shares[:, None, :] * group_marks, axis=2)
    spread = pair_logits[:, 0] - pair_logits[:, 1]
    pair_share = jnp.stack([jax.nn.sigmoid(spread), jax.nn.sigmoid(-spread)], axis=1)
    route_weights = chosen * pair_share
    arrived = lax.all_to_all(send, "ep", split_axis=0, concat_axis=0, tiled=True)
    gate = jnp.einsum("secd,edf->secf", arrived, gate_weight, preferred_element_type=jnp.float32)
    up = jnp.einsum("secd,edf->secf", arrived, up_weight, preferred_element_type=jnp.float32)
    hidden = (jax.nn.silu(gate) * up).astype(jnp.bfloat16)
    result = jnp.einsum(
        "secf,efd->secd",
        lax.all_gather(hidden, "tp", axis=3, tiled=True),
        down_weight,
        preferred_element_type=jnp.float32,
    ).astype(jnp.bfloat16)
    back = lax.all_to_all(result, "ep", split_axis=0, concat_axis=0, tiled=True).reshape(
        EXPERTS, CAP, cols_local
    )
    picked = back[flattened, position].reshape(expert_rows.shape[0], 2, cols_local)
    combined = jnp.sum(route_weights[:, :, None] * picked.astype(jnp.float32), axis=1)
    expert_out = combined.astype(jnp.bfloat16)
    return (mixed, expert_out)


def solution(mesh):
    placed = (
        P("ep", None),
        P(),
        P(None, "tp"),
        P(None, "tp"),
        P(None, "tp"),
        P("tp", "ep"),
        P(None, "tp"),
        P("ep", None),
        P(),
        P("ep", None),
        P("ep", None),
        P("ep", None),
        P("ep", None, "tp"),
        P("ep", None, "tp"),
        P("ep", None, "tp"),
    )
    return jax.shard_map(
        shards,
        mesh=mesh,
        in_specs=placed,
        out_specs=(P("ep", "tp"), P("ep", "tp")),
        check_vma=False,
    )
```

profile of v0, /device:TPU:0, one launch (start us, length us, event | category | flops | bytes accessed | tf_op | source)
XLA Modules:
  0.0 217.6 jit_solution(6197130327097022575)
XLA Ops:
  7.2 0.0 copy-start
  7.2 0.0 all-gather.5.cloned.1.call-start
  7.2 0.9 copy.83
  8.1 0.1 reshape.188
  8.2 0.1 eq.41
  8.4 0.1 eq.45
  8.5 0.6 reduce-window.6
  9.1 0.2 slice_reduce_fusion
  9.4 1.2 fusion.48
  10.6 0.1 fusion.53
  10.7 1.2 fusion.50
  12.0 2.3 %gather_fusion = bf16[256,2048]{1,0:T(8,128)(2,1)} fusion(bf16[128,2048]{1,0:T(8,128)(2,1)S(1)} %fusion.50, s32[1024]{0:T(1024)S(1)} %pad_clamp_fusion), kind=kCustom, calls=%fused_computation | custom fusion | bytes 2098176 | tf_op jit(solution)/shard_map/gather | solution.py:107
  14.3 0.2 broadcast_in_dim.19
  14.6 33.3 %scatter_fusion = bf16[32,16,2048]{2,1,0:T(8,128)(2,1)S(1)} fusion(bf16[32,16,2048]{2,1,0:T(8,128)(2,1)S(1)} %broadcast_in_dim.19, s32[256]{0:T(256)S(1)} %bitcast.90, bf16[256,2048]{1,0:T(8,128)(2,1)} %gather_fusion), kind=kCustom, calls=%fused_computation.2 | custom fusion | bytes 3147776 | tf_op jit(solution)/shard_map/scatter | solution.py:107
  47.9 0.0 slice-start
  47.9 55.4 %all_to_all.10 = bf16[8,4,16,2048]{3,2,1,0:T(8,128)(2,1)S(1)} all-to-all(bf16[8,4,16,2048]{3,2,1,0:T(8,128)(2,1)S(1)} %bitcast.89), channel_id=1, replica_groups=mesh['ep'=8,'tp'=4] {'ep'}, dimensions={0} | all-to-all | bytes 4194304 | tf_op jit(solution)/shard_map/all_to_all | solution.py:118
  103.3 4.8 %fusion.19 = f32[8,4,16,512]{3,2,0,1:T(8,128)S(1)} fusion(bf16[4,2048,512]{2,1,0:T(8,128)(2,1)} %param.29, bf16[8,4,16,2048]{3,2,1,0:T(8,128)(2,1)S(1)} %all_to_all.10), kind=kOutput, calls=%fused_computation.27 | convolution fusion | flops 1073741824 | bytes 11534336 | tf_op jit(solution)/shard_map/secd,edf->secf/dot_general | solution.py:119
  108.1 0.0 slice-done
  108.1 0.0 slice-done.1
  108.1 0.0 copy-start.2
  108.1 0.0 copy-start.7
  108.2 0.0 copy-start.10
  108.2 2.2 fusion.34
  110.3 0.0 all-gather.5.cloned.1.call-update
  110.4 0.0 all-gather.3.cloned.1.call-start
  110.4 0.0 copy-start.8
  110.4 0.2 fusion.45
  110.6 0.0 copy-start.3
  110.6 0.0 copy-start.6
  110.7 0.0 copy-start.5
  110.7 0.3 convolution_convert_fusion.1
  111.0 0.6 copy-done.8
  111.6 0.4 convolution_convert_fusion.2
  112.0 0.7 pad_maximum_fusion
  112.7 0.0 all-gather.3.cloned.1.call-update
  112.7 0.0 copy-done.4
  112.8 0.1 copy.82
  113.0 9.7 %all_gather.13 = bf16[1024,4]{0,1:T(4,128)(2,1)S(1)} all-gather(bf16[128,4]{0,1:T(4,128)(2,1)S(1)} %bitcast.100), channel_id=1, replica_groups=mesh['ep'=8,'tp'=4] {'ep'}, dimensions={0}, use_global_device_ids=true | all-gather | bytes 9216 | tf_op jit(solution)/shard_map/all_gather | solution.py:57
  122.6 21.9 %all-gather.5.cloned.1.call-done = bf16[8,4,16,2048]{3,2,0,1:T(8,128)(2,1)} async-done(((bf16[8,4,16,512]{3,2,0,1:T(8,128)(2,1)}), bf16[8,4,16,2048]{3,2,0,1:T(8,128)(2,1)}) %all-gather.5.cloned.1.call-update) | async-done | bytes 2097168 | tf_op jit(solution)/shard_map/all_gather | solution.py:124
  144.5 5.3 %fusion.42 = bf16[8,4,16,512]{3,2,0,1:T(8,128)(2,1)S(1)} fusion(bf16[8,4,16,2048]{3,2,0,1:T(8,128)(2,1)} %all-gather.5.cloned.1.call-done, bf16[4,2048,512]{2,1,0:T(8,128)(2,1)} %param.31), kind=kOutput, calls=%fused_computation.36 | convolution fusion | flops 1074003968 | bytes 11010048 | tf_op jit(solution)/shard_map/secf,efd->secd/dot_general | solution.py:122
  149.8 0.0 copy-start.9
  149.8 0.9 copy.89
  150.7 4.6 %all-to-all-start.1 = ((bf16[8,4,16,512]{3,2,1,0:T(8,128)(2,1)}), bf16[8,4,16,512]{3,2,1,0:T(8,128)(2,1)}, u32[]{:S(2)}, u32[]{:S(2)}) async-start(bf16[8,4,16,512]{3,2,1,0:T(8,128)(2,1)} %copy.89), calls=%async_computation.1 | async-start | bytes 1048576 | tf_op jit(solution)/shard_map/all_to_all | solution.py:128
  155.3 0.4 convolution_convert_fusion.3
  155.6 19.5 %all-gather.3.cloned.1.call-done = bf16[1024,512]{1,0:T(8,128)(2,1)} async-done(((bf16[128,512]{1,0:T(8,128)(2,1)}), bf16[1024,512]{1,0:T(8,128)(2,1)}) %all-gather.3.cloned.1.call-update) | async-done | bytes 1048592 | tf_op jit(solution)/shard_map/all_gather | solution.py:56
  175.1 17.9 %conditional.1 = (f32[8,4,128]{2,0,1:T(8,128)S(1)}, f32[8,4,128,64]{2,3,1,0:T(8,128)}) conditional(s32[]{:T(128)} %convert_element_type.71, () %tuple.16, (s32[]{:T(128)}, s32[128]{0:T(128)S(1)}, bf16[128,256]{1,0:T(8,128)(2,1)S(1)}, bf16[1024,512]{1,0:T(8,128)(2,1)}, bf16[1024,4]{0,1:T(4,128)(2,1)S(1)}) %tuple.17), branch_computations={%region_1.0_spmd, %region_2.5_spmd} | conditional | flops 217712768 | bytes 26871344 | solution.py:88
  175.1 0.1 copy.79
  175.3 1.5 copy.80
  176.8 0.9 slice_bitcast_fusion
  177.6 0.5 multiply_add_fusion
  178.1 1.8 copy.93
  179.9 2.2 %copy.71 = f32[4,128,8,128]{1,2,3,0:T(8,128)S(1)} copy(f32[4,128,8,128]{3,2,1,0:T(8,128)} %bitcast.93) | data formatting | bytes 4194304 | tf_op jit(solution)/shard_map/cond/branch_1_fun/reshape | solution.py:70
  182.2 0.2 broadcast_compare_fusion
  182.4 1.3 fusion.6
  183.7 7.7 %select_convert_fusion = bf16[4,128,8,128]{1,2,3,0:T(8,128)(2,1)S(1)} fusion(f32[4,128,8,128]{1,2,3,0:T(8,128)S(1)} %copy.71, pred[128,8,128]{0,1,2:T(8,128)(4,1)S(1)} %broadcast_compare_fusion), kind=kOutput, calls=%fused_computation.5 | output fusion | flops 77594624 | bytes 3276800 | tf_op jit(solution)/shard_map/cond/branch_1_fun/reduce_window_sum | solution.py:75
  191.5 0.1 copy.94
  191.6 1.5 fusion.2
  193.1 1.3 multiply_reduce_fusion
  194.5 10.7 %all_gather.14 = bf16[128,1024]{0,1:T(8,128)(2,1)S(1)} all-gather(bf16[128,256]{0,1:T(8,128)(2,1)S(1)} %bitcast.96), channel_id=1, replica_groups=mesh['ep'=8,'tp'=4] {'tp'}, dimensions={1}, use_global_device_ids=true | all-gather | bytes 327680 | tf_op jit(solution)/shard_map/all_gather | solution.py:93
  205.2 1.0 convolution_convert_fusion
  206.2 0.0 all-to-all-done.1
  206.2 2.9 %gather_fusion.1 = bf16[256,512]{1,0:T(8,128)(2,1)S(1)} fusion(bf16[32,16,512]{2,1,0:T(8,128)(2,1)} %bitcast.21, s32[256]{0:T(256)S(1)} %bitcast.91), kind=kCustom, calls=%fused_computation.1 | custom fusion | bytes 526336 | tf_op jit(solution)/shard_map/gather | solution.py:131
  209.0 0.3 reshape.192
  209.4 1.4 multiply_reduce_fusion.1
  (34 shorter events, 0.3 us)
Async XLA Ops:
  7.2 198.0 %copy-start = (bf16[1024,512]{1,0:T(8,128)(2,1)S(1)}, bf16[1024,512]{1,0:T(8,128)(2,1)}, u32[]{:S(2)}) copy-start(bf16[1024,512]{1,0:T(8,128)(2,1)} %param.23) | copy-start | bytes 3145732
  7.2 137.3 %all-gather.5.cloned.1.call-start = ((), (), s32[]{:S(2)}) async-start(), calls=%async_computation.3 | async-start | bytes 2621440 | tf_op jit(solution)/shard_map/all_gather | solution.py:124
  47.9 60.3 %slice-start = ((s8[8388608]{0:T(1024)(128)(4,1)}), s8[4194304]{0:T(1024)(128)(4,1)S(1)}, s32[]{:S(2)}) async-start(s8[8388608]{0:T(1024)(128)(4,1)} %bitcast.102), calls=%async_computation.4 | async-start | bytes 8388608
  103.3 4.8 %slice-start.1 = ((s8[8388608]{0:T(1024)(128)(4,1)}), s8[4194304]{0:T(1024)(128)(4,1)S(1)}, s32[]{:S(2)}) async-start(s8[8388608]{0:T(1024)(128)(4,1)} %bitcast.102), calls=%async_computation.5 | async-start | bytes 8388608
  108.1 2.3 %copy-start.2 = (bf16[128,2048]{1,0:T(8,128)(2,1)S(1)}, bf16[128,2048]{1,0:T(8,128)(2,1)}, u32[]{:S(2)}) copy-start(bf16[128,2048]{1,0:T(8,128)(2,1)} %param.17) | copy-start | bytes 1572868
  108.1 2.5 %copy-start.7 = (bf16[2048,256]{1,0:T(8,128)(2,1)S(1)}, bf16[2048,256]{1,0:T(8,128)(2,1)}, u32[]{:S(2)}) copy-start(bf16[2048,256]{1,0:T(8,128)(2,1)} %param.21) | copy-start | bytes 3145732
  108.2 2.5 %copy-start.10 = (f32[2048]{0:T(1024)S(1)}, f32[2048]{0:T(1024)}, u32[]{:S(2)}) copy-start(f32[2048]{0:T(1024)} %param.18) | copy-start | bytes 24580
  110.4 64.8 %all-gather.3.cloned.1.call-start = ((), (), s32[]{:S(2)}) async-start(), calls=%async_computation.2 | async-start | bytes 1179648 | tf_op jit(solution)/shard_map/all_gather | solution.py:56
  110.4 1.2 copy-start.8
  110.6 2.1 copy-start.4
  110.6 2.1 copy-start.3
  110.6 2.2 copy-start.6
  110.7 2.3 %copy-start.5 = (bf16[4,128]{1,0:T(4,128)(2,1)S(1)}, bf16[4,128]{1,0:T(4,128)(2,1)}, u32[]{:S(2)}) copy-start(bf16[4,128]{1,0:T(4,128)(2,1)} %param.22) | copy-start | bytes 3076
  149.8 5.5 %copy-start.9 = (bf16[2048,256]{1,0:T(8,128)(2,1)S(1)}, bf16[2048,256]{1,0:T(8,128)(2,1)}, u32[]{:S(2)}) copy-start(bf16[2048,256]{1,0:T(8,128)(2,1)} %param.19) | copy-start | bytes 3145732
  150.7 55.5 %all-to-all-start.1 = ((bf16[8,4,16,512]{3,2,1,0:T(8,128)(2,1)}), bf16[8,4,16,512]{3,2,1,0:T(8,128)(2,1)}, u32[]{:S(2)}, u32[]{:S(2)}) async-start(bf16[8,4,16,512]{3,2,1,0:T(8,128)(2,1)} %copy.89), calls=%async_computation.1 | async-start | bytes 1048576 | tf_op jit(solution)/shard_map/all_to_all | solution.py:128
  183.7 7.8 %copy-start.1 = (bf16[32,8,8,128]{3,1,2,0:T(8,128)(2,1)S(1)}, bf16[32,8,8,128]{3,1,2,0:T(8,128)(2,1)}, u32[]{:S(2)}) copy-start(bf16[32,8,8,128]{3,1,2,0:T(8,128)(2,1)} %get-tuple-element.46) | copy-start | bytes 1572868 | tf_op jit(solution)/shard_map/cond
Sparse Core Ops, SparseCore 0:
  110.5 33.9 all-gather.4
  146.7 28.4 all-gather.2
where the time goes:
time: 219 us; the launch traced here: 218 us
  blocking collectives  75.8 us (35%)
  local copies, waits for them, and re-layouts  48.8 us (22%)
  waiting for transfers between devices  41.4 us (19%)
  other arithmetic  16.2 us (7%)
  matrix products  16.2 us (7%)
  between operations  14.4 us (7%)
  starting transfers between devices  4.68 us (2%)
    all_to_all x1, blocking collectives, shards(): lax.all_to_all(send, 'ep', split_axis=0, concat_axis=0, tiled=True)  55.4 us
    scatter x1, local copies, waits for them, and re-layouts, shards(): jnp.zeros((EXPERTS, CAP, width), jnp.bfloat16).at[flattened, position]  33.3 us
    all_gather x1, waiting for transfers between devices, shards(): lax.all_gather(hidden, 'tp', axis=3, tiled=True)  21.9 us
    all_gather x1, waiting for transfers between devices, shards(): lax.all_gather(pairs, 'ep', axis=0, tiled=True)  19.5 us
    all_gather x1, blocking collectives, shards(): lax.all_gather(attended, 'tp', axis=1, tiled=True)  10.7 us
    all_gather x1, blocking collectives, shards(): lax.all_gather(bias_rows, 'ep', axis=0, tiled=True)  9.69 us
    another operation x1, other arithmetic, work(): suffix = lax.cumsum(log_keep, axis=3, reverse=True) - log_keep  7.74 us
    dot_general x1, matrix products, shards(): jnp.einsum('secf,efd->secd', lax.all_gather(hidden, 'tp', axis=3, tiled=T...  5.28 us
  transfers between devices with their start and end apart: 3, of which 2 were waited for; matrix products, arithmetic and copies ran while one was open for 13% of the time, Pallas kernels for 0%

commit v1 on v0

--- a/solution.py
+++ b/solution.py
@@ -121,7 +121,7 @@
     hidden = (jax.nn.silu(gate) * up).astype(jnp.bfloat16)
     result = jnp.einsum(
         "secf,efd->secd",
-        lax.all_gather(hidden, "tp", axis=3, tiled=True),
+        jnp.concatenate(lax.all_gather(hidden, "tp"), axis=3),
         down_weight,
         preferred_element_type=jnp.float32,
     ).astype(jnp.bfloat16)

time: 219 us -> 216 us (0.986)
  waiting for transfers between devices: 41.4 us -> 39.1 us
    all_gather x1, waiting for transfers between devices: 19.5 us -> 17.1 us  [shards(): lax.all_gather(pairs, 'ep', axis=0, tiled=True)]
  transfers between devices with their start and end apart: 3 -> 3, of which waited for: 2 -> 2; matrix products, arithmetic and copies ran while one was open for 13% -> 14% of each run, Pallas kernels for 0% -> 0%
where the time goes in v1:
time: 216 us; the launch traced here: 215 us
  blocking collectives  74.3 us (34%)
  local copies, waits for them, and re-layouts  50.7 us (23%)
  waiting for transfers between devices  39.1 us (18%)
  other arithmetic  16.2 us (8%)
  matrix products  15.7 us (7%)
  between operations  14.4 us (7%)
  starting transfers between devices  4.69 us (2%)
    all_to_all x1, blocking collectives, shards(): lax.all_to_all(send, 'ep', split_axis=0, concat_axis=0, tiled=True)  55.4 us
    scatter x1, local copies, waits for them, and re-layouts, shards(): jnp.zeros((EXPERTS, CAP, width), jnp.bfloat16).at[flattened, position]  33.3 us
    all_gather x1, waiting for transfers between devices, shards(): lax.all_gather(hidden, 'tp')  22 us
    all_gather x1, waiting for transfers between devices, shards(): lax.all_gather(pairs, 'ep', axis=0, tiled=True)  17.1 us
    all_gather x1, blocking collectives, shards(): lax.all_gather(bias_rows, 'ep', axis=0, tiled=True)  9.69 us
    all_gather x1, blocking collectives, shards(): lax.all_gather(attended, 'tp', axis=1, tiled=True)  9.2 us
    another operation x1, other arithmetic, work(): suffix = lax.cumsum(log_keep, axis=3, reverse=True) - log_keep  7.74 us
    dot_general x1, matrix products, shards(): jnp.einsum('secd,edf->secf', arrived, gate_weight, preferred_element_type...  4.79 us
  transfers between devices with their start and end apart: 3, of which 2 were waited for; matrix products, arithmetic and copies ran while one was open for 14% of the time, Pallas kernels for 0%

profile of v1, /device:TPU:0, one launch (start us, length us, event | category | flops | bytes accessed | tf_op | source)
XLA Modules:
  0.0 215.2 jit_solution(4867625466933586362)
XLA Ops:
  7.2 0.0 copy-start
  7.2 0.0 all-gather.6.cloned.1.call-start
  7.2 0.9 copy.86
  8.1 0.1 reshape.194
  8.2 0.1 eq.41
  8.4 0.1 eq.45
  8.5 0.6 reduce-window.6
  9.1 0.2 slice_reduce_fusion
  9.4 1.2 fusion.48
  10.6 0.1 fusion.53
  10.7 1.2 fusion.50
  12.0 2.3 %gather_fusion = bf16[256,2048]{1,0:T(8,128)(2,1)} fusion(bf16[128,2048]{1,0:T(8,128)(2,1)S(1)} %fusion.50, s32[1024]{0:T(1024)S(1)} %pad_clamp_fusion), kind=kCustom, calls=%fused_computation | custom fusion | bytes 2098176 | tf_op jit(solution)/shard_map/gather | solution.py:107
  14.3 0.2 broadcast_in_dim.19
  14.6 33.3 %scatter_fusion = bf16[32,16,2048]{2,1,0:T(8,128)(2,1)S(1)} fusion(bf16[32,16,2048]{2,1,0:T(8,128)(2,1)S(1)} %broadcast_in_dim.19, s32[256]{0:T(256)S(1)} %bitcast.95, bf16[256,2048]{1,0:T(8,128)(2,1)} %gather_fusion), kind=kCustom, calls=%fused_computation.2 | custom fusion | bytes 3147776 | tf_op jit(solution)/shard_map/scatter | solution.py:107
  47.9 0.0 slice-start
  47.9 55.4 %all_to_all.10 = bf16[8,4,16,2048]{3,2,1,0:T(8,128)(2,1)S(1)} all-to-all(bf16[8,4,16,2048]{3,2,1,0:T(8,128)(2,1)S(1)} %bitcast.94), channel_id=1, replica_groups=mesh['ep'=8,'tp'=4] {'ep'}, dimensions={0} | all-to-all | bytes 4194304 | tf_op jit(solution)/shard_map/all_to_all | solution.py:118
  103.3 4.8 %fusion.19 = f32[8,4,16,512]{3,2,0,1:T(8,128)S(1)} fusion(bf16[4,2048,512]{2,1,0:T(8,128)(2,1)} %param.29, bf16[8,4,16,2048]{3,2,1,0:T(8,128)(2,1)S(1)} %all_to_all.10), kind=kOutput, calls=%fused_computation.27 | convolution fusion | flops 1073741824 | bytes 11534336 | tf_op jit(solution)/shard_map/secd,edf->secf/dot_general | solution.py:119
  108.1 0.0 slice-done
  108.1 0.0 slice-done.1
  108.1 0.0 copy-start.2
  108.1 0.0 copy-start.7
  108.2 0.0 copy-start.10
  108.2 2.2 %fusion.34 = bf16[8,4,16,512]{3,2,0,1:T(8,128)(2,1)} fusion(bf16[4,2048,512]{2,1,0:T(8,128)(2,1)S(1)} %bitcast.110, bf16[8,4,16,2048]{3,2,1,0:T(8,128)(2,1)S(1)} %all_to_all.10, f32[8,4,16,512]{3,2,0,1:T(8,128)S(1)} %fusion.19), kind=kOutput, calls=%fused_computation.34 | convolution fusion | flops 1075314688 | bytes 12058624 | tf_op jit(solution)/shard_map/secd,edf->secf/dot_general | solution.py:120
  110.3 0.0 all-gather.6.cloned.1.call-update
  110.4 0.0 all-gather.4.cloned.1.call-start
  110.4 0.0 copy-start.8
  110.4 0.2 fusion.45
  110.6 0.0 copy-start.3
  110.6 0.0 copy-start.6
  110.7 0.0 copy-start.5
  110.7 0.3 convolution_convert_fusion.1
  111.0 0.6 copy-done.8
  111.6 0.4 convolution_convert_fusion.2
  112.0 0.7 pad_maximum_fusion
  112.7 0.0 all-gather.4.cloned.1.call-update
  112.8 0.1 copy.85
  113.0 9.7 %all_gather.16 = bf16[1024,4]{0,1:T(4,128)(2,1)S(1)} all-gather(bf16[128,4]{0,1:T(4,128)(2,1)S(1)} %bitcast.107), channel_id=1, replica_groups=mesh['ep'=8,'tp'=4] {'ep'}, dimensions={0}, use_global_device_ids=true | all-gather | bytes 9216 | tf_op jit(solution)/shard_map/all_gather | solution.py:57
  122.6 22.0 %all-gather.6.cloned.1.call-done = bf16[32,4,16,512]{3,2,0,1:T(8,128)(2,1)} async-done(((bf16[8,4,16,512]{3,2,0,1:T(8,128)(2,1)}), bf16[32,4,16,512]{3,2,0,1:T(8,128)(2,1)}) %all-gather.6.cloned.1.call-update) | async-done | bytes 2097168 | tf_op jit(solution)/shard_map/all_gather | solution.py:124
  144.6 1.9 copy.100
  146.5 4.8 %fusion.42 = bf16[8,4,16,512]{3,2,0,1:T(8,128)(2,1)S(1)} fusion(bf16[8,4,16,2048]{3,2,0,1:T(8,128)(2,1)S(1)} %bitcast.99, bf16[4,2048,512]{2,1,0:T(8,128)(2,1)} %param.31), kind=kOutput, calls=%fused_computation.36 | convolution fusion | flops 1074003968 | bytes 11010048 | tf_op jit(solution)/shard_map/secf,efd->secd/dot_general | solution.py:122
  151.3 0.0 copy-start.9
  151.3 0.9 copy.93
  152.2 4.6 %all-to-all-start.1 = ((bf16[8,4,16,512]{3,2,1,0:T(8,128)(2,1)}), bf16[8,4,16,512]{3,2,1,0:T(8,128)(2,1)}, u32[]{:S(2)}, u32[]{:S(2)}) async-start(bf16[8,4,16,512]{3,2,1,0:T(8,128)(2,1)} %copy.93), calls=%async_computation.1 | async-start | bytes 1048576 | tf_op jit(solution)/shard_map/all_to_all | solution.py:128
  156.8 0.3 convolution_convert_fusion.3
  157.1 17.1 %all-gather.4.cloned.1.call-done = bf16[1024,512]{1,0:T(8,128)(2,1)} async-done(((bf16[128,512]{1,0:T(8,128)(2,1)}), bf16[1024,512]{1,0:T(8,128)(2,1)}) %all-gather.4.cloned.1.call-update) | async-done | bytes 1048592 | tf_op jit(solution)/shard_map/all_gather | solution.py:56
  174.3 17.9 %conditional.1 = (f32[8,4,128]{2,0,1:T(8,128)S(1)}, f32[8,4,128,64]{2,3,1,0:T(8,128)}) conditional(s32[]{:T(128)} %convert_element_type.71, () %tuple.16, (s32[]{:T(128)}, s32[128]{0:T(128)S(1)}, bf16[128,256]{1,0:T(8,128)(2,1)S(1)}, bf16[1024,512]{1,0:T(8,128)(2,1)}, bf16[1024,4]{0,1:T(4,128)(2,1)S(1)}) %tuple.17), branch_computations={%region_1.0_spmd, %region_2.5_spmd} | conditional | flops 217712768 | bytes 26871344 | solution.py:88
  174.3 0.1 copy.82
  174.4 1.5 copy.83
  175.9 0.9 slice_bitcast_fusion
  176.7 0.5 multiply_add_fusion
  177.2 1.8 copy.97
  179.0 2.2 %copy.74 = f32[4,128,8,128]{1,2,3,0:T(8,128)S(1)} copy(f32[4,128,8,128]{3,2,1,0:T(8,128)} %bitcast.98) | data formatting | bytes 4194304 | tf_op jit(solution)/shard_map/cond/branch_1_fun/reshape | solution.py:70
  181.3 0.2 broadcast_compare_fusion
  181.5 1.3 fusion.6
  182.8 7.7 %select_convert_fusion = bf16[4,128,8,128]{1,2,3,0:T(8,128)(2,1)S(1)} fusion(f32[4,128,8,128]{1,2,3,0:T(8,128)S(1)} %copy.74, pred[128,8,128]{0,1,2:T(8,128)(4,1)S(1)} %broadcast_compare_fusion), kind=kOutput, calls=%fused_computation.5 | output fusion | flops 77594624 | bytes 3276800 | tf_op jit(solution)/shard_map/cond/branch_1_fun/reduce_window_sum | solution.py:75
  190.6 0.1 copy.98
  190.7 1.5 fusion.2
  192.2 1.3 multiply_reduce_fusion
  193.6 9.2 %all_gather.17 = bf16[128,1024]{0,1:T(8,128)(2,1)S(1)} all-gather(bf16[128,256]{0,1:T(8,128)(2,1)S(1)} %bitcast.103), channel_id=1, replica_groups=mesh['ep'=8,'tp'=4] {'tp'}, dimensions={1}, use_global_device_ids=true | all-gather | bytes 327680 | tf_op jit(solution)/shard_map/all_gather | solution.py:93
  202.8 1.0 convolution_convert_fusion
  203.8 0.0 all-to-all-done.1
  203.8 2.9 %gather_fusion.1 = bf16[256,512]{1,0:T(8,128)(2,1)S(1)} fusion(bf16[32,16,512]{2,1,0:T(8,128)(2,1)} %bitcast.23, s32[256]{0:T(256)S(1)} %bitcast.96), kind=kCustom, calls=%fused_computation.1 | custom fusion | bytes 526336 | tf_op jit(solution)/shard_map/gather | solution.py:131
  206.6 0.3 reshape.200
  207.0 1.4 multiply_reduce_fusion.1
  (35 shorter events, 0.3 us)
Async XLA Ops:
  7.2 195.6 %copy-start = (bf16[1024,512]{1,0:T(8,128)(2,1)S(1)}, bf16[1024,512]{1,0:T(8,128)(2,1)}, u32[]{:S(2)}) copy-start(bf16[1024,512]{1,0:T(8,128)(2,1)} %param.23) | copy-start | bytes 3145732
  7.2 137.5 %all-gather.6.cloned.1.call-start = ((), (), s32[]{:S(2)}) async-start(), calls=%async_computation.3 | async-start | bytes 2621440 | tf_op jit(solution)/shard_map/all_gather | solution.py:124
  47.9 60.3 %slice-start = ((s8[8388608]{0:T(1024)(128)(4,1)}), s8[4194304]{0:T(1024)(128)(4,1)S(1)}, s32[]{:S(2)}) async-start(s8[8388608]{0:T(1024)(128)(4,1)} %bitcast.109), calls=%async_computation.4 | async-start | bytes 8388608
  103.3 4.8 %slice-start.1 = ((s8[8388608]{0:T(1024)(128)(4,1)}), s8[4194304]{0:T(1024)(128)(4,1)S(1)}, s32[]{:S(2)}) async-start(s8[8388608]{0:T(1024)(128)(4,1)} %bitcast.109), calls=%async_computation.5 | async-start | bytes 8388608
  108.1 2.3 %copy-start.2 = (bf16[128,2048]{1,0:T(8,128)(2,1)S(1)}, bf16[128,2048]{1,0:T(8,128)(2,1)}, u32[]{:S(2)}) copy-start(bf16[128,2048]{1,0:T(8,128)(2,1)} %param.17) | copy-start | bytes 1572868
  108.1 2.5 %copy-start.7 = (bf16[2048,256]{1,0:T(8,128)(2,1)S(1)}, bf16[2048,256]{1,0:T(8,128)(2,1)}, u32[]{:S(2)}) copy-start(bf16[2048,256]{1,0:T(8,128)(2,1)} %param.21) | copy-start | bytes 3145732
  108.2 2.5 %copy-start.10 = (f32[2048]{0:T(1024)S(1)}, f32[2048]{0:T(1024)}, u32[]{:S(2)}) copy-start(f32[2048]{0:T(1024)} %param.18) | copy-start | bytes 24580
  110.4 63.9 %all-gather.4.cloned.1.call-start = ((), (), s32[]{:S(2)}) async-start(), calls=%async_computation.2 | async-start | bytes 1179648 | tf_op jit(solution)/shard_map/all_gather | solution.py:56
  110.4 1.2 copy-start.8
  110.6 2.1 copy-start.4
  110.6 2.1 copy-start.3
  110.6 2.2 %copy-start.6 = (f32[128,2]{0,1:T(2,128)S(1)}, f32[128,2]{0,1:T(2,128)}, u32[]{:S(2)}) copy-start(f32[128,2]{0,1:T(2,128)} %param.28) | copy-start | bytes 3076
  110.7 2.3 %copy-start.5 = (bf16[4,128]{1,0:T(4,128)(2,1)S(1)}, bf16[4,128]{1,0:T(4,128)(2,1)}, u32[]{:S(2)}) copy-start(bf16[4,128]{1,0:T(4,128)(2,1)} %param.22) | copy-start | bytes 3076
  151.3 5.5 %copy-start.9 = (bf16[2048,256]{1,0:T(8,128)(2,1)S(1)}, bf16[2048,256]{1,0:T(8,128)(2,1)}, u32[]{:S(2)}) copy-start(bf16[2048,256]{1,0:T(8,128)(2,1)} %param.19) | copy-start | bytes 3145732
  152.2 51.6 %all-to-all-start.1 = ((bf16[8,4,16,512]{3,2,1,0:T(8,128)(2,1)}), bf16[8,4,16,512]{3,2,1,0:T(8,128)(2,1)}, u32[]{:S(2)}, u32[]{:S(2)}) async-start(bf16[8,4,16,512]{3,2,1,0:T(8,128)(2,1)} %copy.93), calls=%async_computation.1 | async-start | bytes 1048576 | tf_op jit(solution)/shard_map/all_to_all | solution.py:128
  182.8 7.8 %copy-start.1 = (bf16[32,8,8,128]{3,1,2,0:T(8,128)(2,1)S(1)}, bf16[32,8,8,128]{3,1,2,0:T(8,128)(2,1)}, u32[]{:S(2)}) copy-start(bf16[32,8,8,128]{3,1,2,0:T(8,128)(2,1)} %get-tuple-element.46) | copy-start | bytes 1572868 | tf_op jit(solution)/shard_map/cond
Sparse Core Ops, SparseCore 0:
  110.5 34.1 all-gather.5
  146.8 27.4 all-gather.3
